TPU v7x, 32 devices: a whole 2x2x4 slice. The times are simulated.
32 devices in a mesh: ep: 4 (over z), tp: 8 (over y, x, core).
Axes of the slice: x: 2, y: 2, z: 4, core: 2. Of those that a mesh axis runs over, the one named last changes fastest.
Arguments:
- tokens: bfloat16 [512, 2048], P('ep', 'tp'), may hold values from -6 to 6
- out_grad: bfloat16 [512, 2048], P('ep', 'tp'), may hold values from -6 to 6
- routes: int32 [512, 2], P('ep'), may hold values from 0 to 3, all different within a row; in each aligned block of 128 rows (0 to 127, 128 to 255, ...) at most 96 rows name the same one
- gates: float32 [512, 2], P('ep'), may hold values from 0.1 to 0.9
- gate_weight: bfloat16 [4, 2048, 5632], P('ep', None, 'tp'), may hold values from -0.125 to 0.125
- up_weight: bfloat16 [4, 2048, 5632], P('ep', None, 'tp'), may hold values from -0.125 to 0.125
- down_weight: bfloat16 [4, 5632, 2048], P('ep', 'tp'), may hold values from -0.078125 to 0.078125
Outputs:
- tokens_grad: bfloat16 [512, 2048], P('ep', 'tp')
- gates_grad: float32 [512, 2], P(('ep', 'tp'))
- gate_weight_grad: bfloat16 [4, 2048, 5632], P('ep', None, 'tp')
- up_weight_grad: bfloat16 [4, 2048, 5632], P('ep', None, 'tp')
- down_weight_grad: bfloat16 [4, 5632, 2048], P('ep', 'tp')
Inputs may be any that keep to these rules, and one draw needn't show every extreme that they name: `routes`: the 2 experts of a token differ. In each aligned block of 128 rows (the tokens of one index of ep) no expert is named by more than 96 rows, a bound that some block reaches.
All inputs are finite; a program needn't handle non-finite values.
Results may differ from a plain program's by a relative error of at most 0.029.
Values may be sent and summed in bfloat16 or wider, within the bound.
A program may use at most 64 MiB of HBM per device.

v0:
```python
import jax
import jax.numpy as jnp
from jax import lax
from jax.sharding import PartitionSpec as P


def expert_grads(rows, cotan, w_gate, w_up, w_down):
    pre_gate = jnp.dot(rows, w_gate, preferred_element_type=jnp.float32)
    pre_up = jnp.dot(rows, w_up, preferred_element_type=jnp.float32)
    activated = jax.nn.silu(pre_gate)
    hidden = (activated * pre_up).astype(jnp.bfloat16)
    hid_grad = jnp.dot(cotan, w_down.T, preferred_element_type=jnp.float32)
    sigmoid_gate = jax.nn.sigmoid(pre_gate)
    gate_part = (hid_grad * pre_up * sigmoid_gate * (1.0 + pre_gate * (1.0 - sigmoid_gate))).astype(
        jnp.bfloat16
    )
    up_part = (hid_grad * activated).astype(jnp.bfloat16)
    slot_dots = jnp.sum(hidden.astype(jnp.float32) * hid_grad, axis=1)
    down_grad = jnp.dot(hidden.T, cotan, preferred_element_type=jnp.float32).astype(jnp.bfloat16)
    gate_grad = jnp.dot(rows.T, gate_part, preferred_element_type=jnp.float32).astype(jnp.bfloat16)
    up_grad = jnp.dot(rows.T, up_part, preferred_element_type=jnp.float32).astype(jnp.bfloat16)
    return (gate_part, up_part, slot_dots, gate_grad, up_grad, down_grad)


def on_device(tokens, out_grad, routes, gates, gate_weight, up_weight, down_weight):
    tok_dev, top_k = routes.shape
    ep_size = lax.axis_size("ep")
    tp_size = lax.axis_size("tp")
    capacity = (3 * tok_dev + ep_size - 1) // ep_size
    buffer_rows = ep_size * capacity
    slice_width = tokens.shape[1]
    flat_expert = routes.reshape(-1)
    onehot = (flat_expert[:, None] == jnp.arange(ep_size, dtype=jnp.int32)[None, :]).astype(
        jnp.int32
    )
    slot_rank = jnp.sum((jnp.cumsum(onehot, axis=0) - onehot) * onehot, axis=1)
    slot_dest = flat_expert * capacity + slot_rank
    placed = jnp.arange(buffer_rows, dtype=jnp.int32)[:, None] == slot_dest[None, :]
    placed_float = placed.astype(jnp.float32)
    select = jnp.any(placed.reshape(buffer_rows, tok_dev, top_k), axis=2).astype(jnp.bfloat16)
    slot_gate = jnp.dot(placed_float, gates.reshape(-1), precision=lax.Precision.HIGHEST)
    sent_rows = jnp.dot(select, tokens, preferred_element_type=jnp.float32).astype(jnp.bfloat16)
    cotan_rows = jnp.dot(select, out_grad, preferred_element_type=jnp.float32)
    sent_cotan = (slot_gate[:, None] * cotan_rows).astype(jnp.bfloat16)
    recv_rows, recv_cotan = (
        lax.all_to_all(
            sent_rows.reshape(ep_size, capacity, slice_width),
            "ep",
            split_axis=0,
            concat_axis=0,
            tiled=True,
        ),
        lax.all_to_all(
            sent_cotan.reshape(ep_size, capacity, slice_width),
            "ep",
            split_axis=0,
            concat_axis=0,
            tiled=True,
        ),
    )
    whole_rows, whole_cotan = (
        lax.all_gather(recv_rows, "tp", axis=2, tiled=True),
        lax.all_gather(recv_cotan, "tp", axis=2, tiled=True),
    )
    model_width = whole_rows.shape[2]
    rows = whole_rows.reshape(buffer_rows, model_width)
    cotan = whole_cotan.reshape(buffer_rows, model_width)
    w_gate = gate_weight[0]
    w_up = up_weight[0]
    gate_part, up_part, slot_dots, gate_grad, up_grad, down_grad = expert_grads(
        rows, cotan, w_gate, w_up, down_weight[0]
    )
    partial_value = jnp.dot(gate_part, w_gate.T, preferred_element_type=jnp.float32)
    partial_value = (
        partial_value + jnp.dot(up_part, w_up.T, preferred_element_type=jnp.float32)
    ).astype(jnp.bfloat16)
    share = tok_dev // tp_size
    start = lax.axis_index("tp") * share
    summed = lax.psum(slot_dots, "tp")
    row_sums = lax.psum_scatter(
        partial_value.reshape(ep_size, capacity, model_width), "tp", scatter_dimension=2, tiled=True
    ).astype(jnp.float32)
    back_rows, back_dots = (
        lax.all_to_all(
            row_sums.astype(jnp.bfloat16), "ep", split_axis=0, concat_axis=0, tiled=True
        ).astype(row_sums.dtype),
        lax.all_to_all(
            summed.reshape(ep_size, capacity).astype(jnp.bfloat16),
            "ep",
            split_axis=0,
            concat_axis=0,
            tiled=True,
        ).astype(jnp.float32),
    )
    slot_rows = back_rows.reshape(buffer_rows, slice_width)[slot_dest]
    tokens_grad = jnp.sum(slot_rows.reshape(tok_dev, top_k, slice_width), axis=1).astype(
        jnp.bfloat16
    )
    token_dots = back_dots.reshape(buffer_rows)[slot_dest].reshape(tok_dev, top_k)
    own_dots = lax.dynamic_slice_in_dim(token_dots, start, share, 0)
    own_gates = lax.dynamic_slice_in_dim(gates, start, share, 0)
    gates_grad = own_dots / own_gates
    return (tokens_grad, gates_grad, gate_grad[None], up_grad[None], down_grad[None])


def solution(mesh):
    placed = (
        P("ep", "tp"),
        P("ep", "tp"),
        P("ep", None),
        P("ep", None),
        P("ep", None, "tp"),
        P("ep", None, "tp"),
        P("ep", "tp", None),
    )
    return jax.shard_map(
        on_device,
        mesh=mesh,
        in_specs=placed,
        out_specs=(
            P("ep", "tp"),
            P(("ep", "tp"), None),
            P("ep", None, "tp"),
            P("ep", None, "tp"),
            P("ep", "tp", None),
        ),
        check_vma=False,
    )
```

profile of v0, /device:TPU:0, one launch (start us, length us, event | category | flops | bytes accessed | tf_op | source)
XLA Modules:
  0.0 148.4 jit_solution(13399779016683613916)
XLA Ops:
  7.2 0.0 copy-start
  7.2 0.0 copy-start.6
  7.2 0.0 copy-start.5
  7.2 0.0 all-gather.5.cloned.1.call-start
  7.2 0.9 copy.32
  8.2 0.1 eq.47
  8.3 0.1 reshape.125
  8.5 1.2 reduce-window.6
  9.7 0.1 slice.12
  9.8 0.1 copy.34
  9.9 0.1 copy.35
  10.0 0.1 add_bitcast_fusion
  10.1 0.1 reduce_sum.32
  10.3 0.6 broadcast_multiply_fusion
  10.9 0.1 copy.38
  11.0 0.1 fusion.17
  11.0 1.0 convolution_convert_fusion.3
  12.1 13.7 %all_to_all.21 = bf16[4,96,256]{2,1,0:T(8,128)(2,1)} all-to-all(bf16[4,96,256]{2,1,0:T(8,128)(2,1)S(1)} %bitcast.70), channel_id=1, replica_groups=mesh['ep'=4,'tp'=8] {'ep'}, dimensions={0} | all-to-all | bytes 393216 | tf_op jit(solution)/shard_map/all_to_all | solution.py:46
  25.8 0.0 all-gather.5.cloned.1.call-update
  25.8 0.0 all-gather.3.cloned.1.call-start
  25.9 0.0 copy-done.6
  25.9 0.1 copy.36
  26.0 0.1 reshape.156
  26.2 0.3 convolution_reduce_fusion
  26.5 0.0 copy-done.5
  26.5 0.2 fusion.15
  26.7 9.9 %all_to_all.22 = bf16[4,96,256]{2,1,0:T(8,128)(2,1)} all-to-all(bf16[4,96,256]{2,1,0:T(8,128)(2,1)S(1)} %bitcast.69), channel_id=1, replica_groups=mesh['ep'=4,'tp'=8] {'ep'}, dimensions={0} | all-to-all | bytes 393216 | tf_op jit(solution)/shard_map/all_to_all | solution.py:53
  36.6 0.0 all-gather.3.cloned.1.call-update
  36.6 0.0 reduce-scatter.2.cloned.1.call-start
  36.6 14.2 %all-gather.5.cloned.1.call-done = bf16[4,96,2048]{2,1,0:T(8,128)(2,1)} async-done(((bf16[4,96,256]{2,1,0:T(8,128)(2,1)}), bf16[4,96,2048]{2,1,0:T(8,128)(2,1)}) %all-gather.5.cloned.1.call-update) | async-done | bytes 1572880 | tf_op jit(solution)/shard_map/all_gather | solution.py:62
  50.9 0.0 copy-done
  50.9 0.0 copy-start.7
  50.9 4.2 %fusion.5 = f32[384,704]{0,1:T(8,128)} fusion(bf16[384,2048]{1,0:T(8,128)(2,1)} %bitcast.74, bf16[1,2048,704]{1,2,0:T(8,128)(2,1)S(1)} %copy-done), kind=kOutput, calls=%fused_computation.11 | convolution fusion | flops 1107296256 | bytes 5537792 | tf_op jit(solution)/shard_map/dot_general | solution.py:8
  55.1 0.0 copy-done.1
  55.1 0.0 copy-done.7
  55.1 2.7 %fusion.9 = f32[384,704]{0,1:T(8,128)} fusion(bf16[384,2048]{1,0:T(8,128)(2,1)S(1)} %bitcast.76, bf16[1,2048,704]{1,2,0:T(8,128)(2,1)S(1)} %copy-done.1), kind=kOutput, calls=%fused_computation.15 | convolution fusion | flops 1107296256 | bytes 5537792 | tf_op jit(solution)/shard_map/dot_general | solution.py:9
  57.8 20.8 %all-gather.3.cloned.1.call-done = bf16[4,96,2048]{2,1,0:T(8,128)(2,1)} async-done(((bf16[4,96,256]{2,1,0:T(8,128)(2,1)}), bf16[4,96,2048]{2,1,0:T(8,128)(2,1)}) %all-gather.3.cloned.1.call-update) | async-done | bytes 1572880 | tf_op jit(solution)/shard_map/all_gather | solution.py:63
  78.6 5.7 %multiply_reduce_fusion = (f32[384]{0:T(512)S(1)}, bf16[384,704]{0,1:T(8,128)(2,1)}, bf16[384,704]{0,1:T(8,128)(2,1)S(1)}, bf16[384,704]{0,1:T(8,128)(2,1)S(1)}) fusion(f32[384,704]{0,1:T(8,128)} %fusion.9, f32[384,704]{0,1:T(8,128)} %fusion.5, bf16[384,2048]{1,0:T(8,128)(2,1)} %bitcast.78, bf16[1,704,2048]{2,1,0:T(8,128)(2,1)} %param.13), kind=kOutput, calls=%fused_computation.23 | convolution fusion | flops 1112161920 | bytes 8242688 | tf_op jit(solution)/shard_map/dot_general | solution.py:12
  84.3 0.0 copy-start.3
  84.3 1.4 fusion.3
  85.7 0.0 copy-done.3
  85.8 0.6 copy-done.2
  86.3 2.6 %add_convert_fusion = bf16[384,2048]{1,0:T(8,128)(2,1)} fusion(f32[384,2048]{1,0:T(8,128)S(1)} %fusion.3, bf16[384,704]{0,1:T(8,128)(2,1)S(1)} %get-tuple-element.23, bf16[1,2048,704]{1,2,0:T(8,128)(2,1)S(1)} %copy-done.2), kind=kOutput, calls=%fused_computation.5 | convolution fusion | flops 1108869120 | bytes 8142848 | tf_op jit(solution)/shard_map/dot_general | solution.py:75
  89.0 0.0 reduce-scatter.2.cloned.1.call-update
  89.0 1.0 mul.77
  90.0 13.1 %psum.7 = bf16[384]{0:T(512)(128)(2,1)S(1)} all-reduce(f32[384]{0:T(512)S(1)} %get-tuple-element.20), channel_id=1, replica_groups=mesh['ep'=4,'tp'=8] {'tp'}, use_global_device_ids=true, to_apply=%region_7.8 | all-reduce | flops 384 | bytes 2304 | tf_op jit(solution)/shard_map/psum | solution.py:79
  103.1 0.7 convert_element_type.83
  103.8 4.6 %all-to-all-start.3 = ((bf16[4,1,96]{2,1,0:T(2,128)(2,1)}), bf16[4,1,96]{2,1,0:T(2,128)(2,1)S(1)}, u32[]{:S(2)}, u32[]{:S(2)}) async-start(bf16[4,1,96]{2,1,0:T(2,128)(2,1)} %convert_element_type.83), calls=%async_computation.4 | async-start | bytes 4096 | tf_op jit(solution)/shard_map/all_to_all | solution.py:87
  108.4 5.0 %fusion.1 = bf16[1,2048,704]{1,2,0:T(8,128)(2,1)} fusion(bf16[384,704]{0,1:T(8,128)(2,1)S(1)} %get-tuple-element.22, bf16[384,2048]{1,0:T(8,128)(2,1)} %bitcast.75), kind=kOutput, calls=%fused_computation.7 | convolution fusion | flops 1108738048 | bytes 4997120 | tf_op jit(solution)/shard_map/dot_general | solution.py:20
  113.4 0.0 copy-done.4
  113.4 0.0 copy-done.8
  113.4 3.2 %fusion.2 = bf16[1,2048,704]{1,2,0:T(8,128)(2,1)} fusion(bf16[384,704]{0,1:T(8,128)(2,1)S(1)} %copy-done.4, bf16[384,2048]{1,0:T(8,128)(2,1)S(1)} %bitcast.77), kind=kOutput, calls=%fused_computation.8 | convolution fusion | flops 1108738048 | bytes 4997120 | tf_op jit(solution)/shard_map/dot_general | solution.py:21
  116.7 0.0 all-to-all-done.3
  116.7 10.8 %reduce-scatter.2.cloned.1.call-done = bf16[4,96,256]{2,1,0:T(8,128)(2,1)} async-done(((bf16[4,96,2048]{2,1,0:T(8,128)(2,1)}), bf16[4,96,256]{2,1,0:T(8,128)(2,1)}) %reduce-scatter.2.cloned.1.call-update) | async-done | bytes 196624 | tf_op jit(solution)/shard_map/reduce_scatter | solution.py:80
  127.5 4.6 %all-to-all-start.2 = ((bf16[4,96,256]{2,1,0:T(8,128)(2,1)}), bf16[4,96,256]{2,1,0:T(8,128)(2,1)S(1)}, u32[]{:S(2)}, u32[]{:S(2)}) async-start(bf16[4,96,256]{2,1,0:T(8,128)(2,1)} %reduce-scatter.2.cloned.1.call-done), calls=%async_computation.3 | async-start | bytes 393216 | tf_op jit(solution)/shard_map/all_to_all | solution.py:84
  132.1 4.8 %fusion = bf16[1,704,2048]{2,1,0:T(8,128)(2,1)} fusion(bf16[384,704]{0,1:T(8,128)(2,1)} %get-tuple-element.21, bf16[384,2048]{1,0:T(8,128)(2,1)} %bitcast.79), kind=kOutput, calls=%fused_computation.6 | convolution fusion | flops 1108738048 | bytes 4997120 | tf_op jit(solution)/shard_map/dot_general | solution.py:19
  136.9 0.1 reshape.139
  137.0 1.9 %gather_fusion.1 = f32[256]{0:T(256)S(1)} fusion(f32[384]{0:T(512)S(1)} %reshape.139, s32[1024]{0:T(1024)S(1)} %pad_clamp_fusion), kind=kCustom, calls=%fused_computation.1 | custom fusion | bytes 3072 | tf_op jit(solution)/shard_map/gather | solution.py:99
  139.0 0.1 reshape.136
  139.1 0.6 copy.41
  139.8 0.0 all-to-all-done.2
  139.8 1.0 gather_fusion
  140.8 0.1 reshape.135
  140.9 0.9 reduce_sum.34
  (14 shorter events, 0.2 us)
Async XLA Ops:
  7.2 43.7 %copy-start = (bf16[1,2048,704]{1,2,0:T(8,128)(2,1)S(1)}, bf16[1,2048,704]{1,2,0:T(8,128)(2,1)}, u32[]{:S(2)}) copy-start(bf16[1,2048,704]{1,2,0:T(8,128)(2,1)} %param.11) | copy-start | bytes 8650756
  7.2 18.7 %copy-start.6 = (f32[128,2]{0,1:T(2,128)S(1)}, f32[128,2]{0,1:T(2,128)}, u32[]{:S(2)}) copy-start(f32[128,2]{0,1:T(2,128)} %param.10) | copy-start | bytes 3076
  7.2 19.3 %copy-start.5 = (bf16[128,256]{1,0:T(8,128)(2,1)S(1)}, bf16[128,256]{1,0:T(8,128)(2,1)}, u32[]{:S(2)}) copy-start(bf16[128,256]{1,0:T(8,128)(2,1)} %param.8) | copy-start | bytes 196612
  7.2 43.7 %all-gather.5.cloned.1.call-start = ((), (), s32[]{:S(2)}) async-start(), calls=%async_computation.6 | async-start | bytes 1769472 | tf_op jit(solution)/shard_map/all_gather | solution.py:62
  25.8 52.7 %all-gather.3.cloned.1.call-start = ((), (), s32[]{:S(2)}) async-start(), calls=%async_computation.5 | async-start | bytes 1769472 | tf_op jit(solution)/shard_map/all_gather | solution.py:63
  36.6 90.9 %reduce-scatter.2.cloned.1.call-start = ((), (), s32[]{:S(2)}) async-start(), calls=%async_computation.7 | async-start | bytes 1769472 | tf_op jit(solution)/shard_map/reduce_scatter | solution.py:80
  50.9 4.2 %copy-start.1 = (bf16[1,2048,704]{1,2,0:T(8,128)(2,1)S(1)}, bf16[1,2048,704]{1,2,0:T(8,128)(2,1)}, u32[]{:S(2)}) copy-start(bf16[1,2048,704]{1,2,0:T(8,128)(2,1)} %param.12) | copy-start | bytes 8650756
  50.9 4.2 %copy-start.7 = (bf16[4,96,2048]{2,1,0:T(8,128)(2,1)S(1)}, bf16[4,96,2048]{2,1,0:T(8,128)(2,1)}, u32[]{:S(2)}) copy-start(bf16[4,96,2048]{2,1,0:T(8,128)(2,1)} %all-gather.5.cloned.1.call-done) | copy-start | bytes 4718596
  84.3 1.4 copy-start.3
  84.3 2.0 %copy-start.2 = (bf16[1,2048,704]{1,2,0:T(8,128)(2,1)S(1)}, bf16[1,2048,704]{1,2,0:T(8,128)(2,1)}, u32[]{:S(2)}) copy-start(bf16[1,2048,704]{1,2,0:T(8,128)(2,1)} %param.12) | copy-start | bytes 8650756
  103.8 12.9 %all-to-all-start.3 = ((bf16[4,1,96]{2,1,0:T(2,128)(2,1)}), bf16[4,1,96]{2,1,0:T(2,128)(2,1)S(1)}, u32[]{:S(2)}, u32[]{:S(2)}) async-start(bf16[4,1,96]{2,1,0:T(2,128)(2,1)} %convert_element_type.83), calls=%async_computation.4 | async-start | bytes 4096 | tf_op jit(solution)/shard_map/all_to_all | solution.py:87
  108.4 5.0 %copy-start.4 = (bf16[384,704]{0,1:T(8,128)(2,1)S(1)}, bf16[384,704]{0,1:T(8,128)(2,1)}, u32[]{:S(2)}) copy-start(bf16[384,704]{0,1:T(8,128)(2,1)} %copy-done.3) | copy-start | bytes 1622020
  108.4 5.0 %copy-start.8 = (bf16[4,96,2048]{2,1,0:T(8,128)(2,1)S(1)}, bf16[4,96,2048]{2,1,0:T(8,128)(2,1)}, u32[]{:S(2)}) copy-start(bf16[4,96,2048]{2,1,0:T(8,128)(2,1)} %all-gather.5.cloned.1.call-done) | copy-start | bytes 4718596
  127.5 12.3 %all-to-all-start.2 = ((bf16[4,96,256]{2,1,0:T(8,128)(2,1)}), bf16[4,96,256]{2,1,0:T(8,128)(2,1)S(1)}, u32[]{:S(2)}, u32[]{:S(2)}) async-start(bf16[4,96,256]{2,1,0:T(8,128)(2,1)} %reduce-scatter.2.cloned.1.call-done), calls=%async_computation.3 | async-start | bytes 393216 | tf_op jit(solution)/shard_map/all_to_all | solution.py:84
Sparse Core Ops, SparseCore 0:
  26.0 24.8 all-gather.4
  52.8 25.7 all-gather.2
  89.1 38.3 reduce-scatter.1
where the time goes:
time: 149 us; the launch traced here: 148 us
  waiting for transfers between devices  45.9 us (31%)
  blocking collectives  36.7 us (25%)
  matrix products  31.3 us (21%)
  between operations  13.9 us (9%)
  starting transfers between devices  9.33 us (6%)
  local copies, waits for them, and re-layouts  8.1 us (5%)
  other arithmetic  3.1 us (2%)
    all_gather x1, waiting for transfers between devices, on_device(): lax.all_gather(recv_cotan, 'tp', axis=2, tiled=True)  20.8 us
    all_gather x1, waiting for transfers between devices, on_device(): lax.all_gather(recv_rows, 'tp', axis=2, tiled=True)  14.2 us
    all_to_all x1, blocking collectives, on_device(): lax.all_to_all(sent_rows.reshape(ep_size, capacity, slice_width), 'ep', s...  13.7 us
    psum x1, blocking collectives, on_device(): summed = lax.psum(slot_dots, 'tp')  13.1 us
    reduce_scatter x1, waiting for transfers between devices, on_device(): lax.psum_scatter(partial_value.reshape(ep_size, capacity, model_width), '...  10.8 us
    all_to_all x1, blocking collectives, on_device(): lax.all_to_all(sent_cotan.reshape(ep_size, capacity, slice_width), 'ep',...  9.87 us
    dot_general x1, matrix products, expert_grads(): hid_grad = jnp.dot(cotan, w_down.T, preferred_element_type=jnp.float32)  5.73 us
    dot_general x1, matrix products, expert_grads(): jnp.dot(rows.T, gate_part, preferred_element_type=jnp.float32)  5.03 us
  transfers between devices with their start and end apart: 5, of which 3 were waited for; matrix products, arithmetic and copies ran while one was open for 17% of the time, Pallas kernels for 0%

commit v1 on v0

--- a/solution.py
+++ b/solution.py
@@ -1,7 +1,401 @@
+import functools
+
 import jax
 import jax.numpy as jnp
 from jax import lax
+from jax.experimental import pallas as pl
+from jax.experimental.pallas import tpu as pltpu
 from jax.sharding import PartitionSpec as P
+
+MESH = pl.DeviceIdType.MESH
+BF16 = jnp.bfloat16
+F32 = jnp.float32
+VMEM_BYTES = 60 * 1024 * 1024
+
+
+def dot_nn(a, b):
+    return lax.dot_general(a, b, (((1,), (0,)), ((), ())), preferred_element_type=F32)
+
+
+def dot_nt(a, b):
+    return lax.dot_general(a, b, (((1,), (1,)), ((), ())), preferred_element_type=F32)
+
+
+def dot_tn(a, b):
+    return lax.dot_general(a, b, (((0,), (0,)), ((), ())), preferred_element_type=F32)
+
+
+def flip(t, bit):
+    return t + bit - 2 * bit * lax.rem(lax.div(t, bit), 2)
+
+
+def exchange_kernel(
+    ep, tp, cap,
+    tok_ref, og_ref, routes_ref, gates_ref, wg_hbm, wu_hbm, wd_hbm,
+    tg_ref, gg_ref, xo_hbm, co_hbm, ho_hbm, gpo_hbm, upo_hbm,
+    wg, wu, wd, sx, sc, xs, cs, comb_ref, dest_ref,
+    pg, pu, hg, hid, gp, up,
+    psib, rsib, pown, rown, mine, tsum, back, dsend, drecv, dsum, dback,
+    wsem, osem,
+    zs, zr, ns, nr, ds_, dr, ss, sr,
+    bss, bsr, rs, rr, zbs, zbr, dts, dtr, dzs, dzr,
+):
+    me_e = lax.axis_index("ep")
+    me_t = lax.axis_index("tp")
+    sib = flip(me_t, 1)
+    nbr = (flip(me_t, 2), flip(me_t, 4))
+    diag = flip(nbr[0], 4)
+    slots = ep * cap
+    tok_dev, dw = tok_ref.shape
+    fw = wg.shape[1]
+
+    def rdma(src, dst, s_sem, r_sem, e, t):
+        return pltpu.make_async_remote_copy(
+            src_ref=src, dst_ref=dst, send_sem=s_sem, recv_sem=r_sem,
+            device_id={"ep": e, "tp": t}, device_id_type=MESH,
+        )
+
+    loads = [
+        pltpu.make_async_copy(src.at[0], dst, wsem.at[i])
+        for i, (src, dst) in enumerate(((wg_hbm, wg), (wu_hbm, wu), (wd_hbm, wd)))
+    ]
+    for load in loads:
+        load.start()
+
+    barrier = pltpu.get_barrier_semaphore()
+    for r in range(1, ep):
+        pl.semaphore_signal(
+            barrier, inc=1, device_id={"ep": lax.rem(me_e + r, ep), "tp": me_t}, device_id_type=MESH)
+    for r in range(1, tp):
+        pl.semaphore_signal(
+            barrier, inc=1, device_id={"ep": me_e, "tp": lax.rem(me_t + r, tp)}, device_id_type=MESH)
+
+    expert = [routes_ref[:, k : k + 1].astype(F32) for k in range(2)]
+    lane = lax.broadcasted_iota(jnp.int32, (tok_dev, 128), 1).astype(F32)
+    oh = [jnp.where(expert[k] == lane, 1.0, 0.0) for k in range(2)]
+    row_id = lax.broadcasted_iota(jnp.int32, (tok_dev, tok_dev), 0)
+    col_id = lax.broadcasted_iota(jnp.int32, (tok_dev, tok_dev), 1)
+    below = jnp.where(col_id < row_id, 1.0, 0.0).astype(BF16)
+    before = dot_nn(below, (oh[0] + oh[1]).astype(BF16))
+    rank = [
+        jnp.sum(before * oh[0], axis=1, keepdims=True),
+        jnp.sum((before + oh[0]) * oh[1], axis=1, keepdims=True),
+    ]
+    slot_id = lax.broadcasted_iota(jnp.int32, (tok_dev, slots), 1).astype(F32)
+    dest = [expert[k] * float(cap) + rank[k] for k in range(2)]
+    comb = [jnp.where(dest[k] == slot_id, 1.0, 0.0) for k in range(2)]
+    both = (comb[0] + comb[1]).astype(BF16)
+    comb_ref[...] = both
+    for k in range(2):
+        dest_ref[k] = jnp.broadcast_to(dest[k], (tok_dev, 128))
+    sx[...] = dot_tn(both, tok_ref[...]).astype(BF16)
+    og = og_ref[...].astype(F32)
+    scaled = jnp.concatenate([(gates_ref[:, k : k + 1] * og).astype(BF16) for k in range(2)], axis=0)
+    picks = jnp.concatenate([comb[0], comb[1]], axis=0).astype(BF16)
+    sc[...] = dot_tn(picks, scaled).astype(BF16)
+
+    pl.semaphore_wait(barrier, ep - 1 + tp - 1)
+
+    def rows_of(s):
+        return pl.ds(pl.multiple_of(s * cap, cap), cap)
+
+    sent, big = (sx, sc), (xs, cs)
+    src_of = [lax.rem(me_e + ep - r, ep) for r in range(ep)]
+    n_chunk = 2 * ep
+    sends = []
+
+    def start(copy):
+        copy.start()
+        sends.append(copy)
+        return copy
+
+    z_copy = {}
+    for a in range(2):
+        for r in range(1, ep):
+            to = lax.rem(me_e + r, ep)
+            z_copy[a * ep + r] = start(rdma(
+                sent[a].at[rows_of(to)], big[a].at[me_t, rows_of(me_e)],
+                zs.at[a * ep + r], zr.at[a * ep + r], to, me_t))
+    for a in range(2):
+        big[a][me_t, rows_of(me_e), :] = sent[a][rows_of(me_e), :]
+
+    n_copy, d_copy, s_copy = {}, {}, {}
+
+    def chunk(i, t):
+        return big[i // ep].at[t, rows_of(src_of[i % ep])]
+
+    def to_sibling(i, kind, t):
+        s_copy[i, kind] = start(rdma(
+            chunk(i, t), chunk(i, t), ss.at[i * 4 + kind], sr.at[i * 4 + kind], me_e, sib))
+
+    def stage_a(i):
+        if i in z_copy:
+            z_copy[i].wait_recv()
+        for d in range(2):
+            n_copy[i, d] = start(rdma(
+                chunk(i, me_t), chunk(i, me_t), ns.at[i * 2 + d], nr.at[i * 2 + d], me_e, nbr[d]))
+        to_sibling(i, 0, me_t)
+
+    def stage_b(i):
+        for d in range(2):
+            n_copy[i, d].wait_recv()
+            if i % 2 == d:
+                d_copy[i] = start(rdma(
+                    chunk(i, nbr[d]), chunk(i, nbr[d]), ds_.at[i], dr.at[i], me_e, nbr[1 - d]))
+            to_sibling(i, 1 + d, nbr[d])
+
+    def stage_c(i):
+        d_copy[i].wait_recv()
+        to_sibling(i, 3, diag)
+
+    def settle(a):
+        for i in range(a * ep, (a + 1) * ep):
+            for kind in range(4):
+                s_copy[i, kind].wait_recv()
+
+    def first_half(lo, hi):
+        @pl.loop(lo, hi)
+        def _(j):
+            part = pl.ds(pl.multiple_of(j * dw, dw), dw)
+            x = xs[j]
+            pg[...] += dot_nn(x, wg[part, :])
+            pu[...] += dot_nn(x, wu[part, :])
+
+    outs = []
+
+    def put(src, dst, k):
+        copy = pltpu.make_async_copy(src, dst, osem.at[k])
+        copy.start()
+        outs.append(copy)
+
+    pg[...] = jnp.zeros_like(pg)
+    pu[...] = jnp.zeros_like(pu)
+    hg[...] = jnp.zeros_like(hg)
+    for i in range(n_chunk + 2):
+        if i < n_chunk:
+            stage_a(i)
+        if 1 <= i <= n_chunk:
+            stage_b(i - 1)
+        if i >= 2:
+            stage_c(i - 2)
+        late = i - (ep + 2)
+        if late == 0:
+            settle(0)
+            put(xs, xo_hbm, 0)
+            loads[0].wait()
+            loads[1].wait()
+        if late >= 0:
+            first_half(late * tp // ep, (late + 1) * tp // ep)
+    settle(1)
+    put(cs, co_hbm, 1)
+    loads[2].wait()
+
+    @pl.loop(0, tp)
+    def _(j):
+        part = pl.ds(pl.multiple_of(j * dw, dw), dw)
+        hg[...] += dot_nt(cs[j], wd[:, part])
+
+    block = 16
+
+    @pl.loop(0, slots // block)
+    def _(b):
+        at = pl.ds(pl.multiple_of(b * block, block), block)
+        g, u, h = pg[at, :], pu[at, :], hg[at, :]
+        sig = jax.nn.sigmoid(g)
+        act = g * sig
+        hidden = (act * u).astype(BF16)
+        hid[at, :] = hidden
+        gp[at, :] = (h * u * sig * (1.0 + g * (1.0 - sig))).astype(BF16)
+        up[at, :] = (h * act).astype(BF16)
+        pg[at, :] = hidden.astype(F32) * h
+
+    put(hid, ho_hbm, 2)
+    put(gp, gpo_hbm, 3)
+    put(up, upo_hbm, 4)
+
+    def piece(t):
+        part = pl.ds(pl.multiple_of(t * dw, dw), dw)
+        return dot_nt(gp[...], wg[part, :]) + dot_nt(up[...], wu[part, :])
+
+    chips = (diag, nbr[0], nbr[1], me_t)
+    b_copy = []
+    for q in range(4):
+        psib[q] = piece(flip(chips[q], 1)).astype(BF16)
+        b_copy.append(start(rdma(psib.at[q], rsib.at[q], bss.at[q], bsr.at[q], me_e, sib)))
+    for q in range(3):
+        own = piece(chips[q])
+        b_copy[q].wait_recv()
+        pown[q] = (own + rsib[q].astype(F32)).astype(BF16)
+    order = list(range(1, ep)) + [0]
+    r_copy = {}
+    for r in order:
+        for q in range(3):
+            at = rows_of(lax.rem(me_e + r, ep))
+            r_copy[r, q] = start(rdma(
+                pown.at[q, at], rown.at[q, at], rs.at[r * 3 + q], rr.at[r * 3 + q], me_e, chips[q]))
+
+    ones = jnp.ones((8, fw), F32)
+    for s in range(ep):
+        dsend[s] = lax.dot_general(
+            ones, pg[s * cap : (s + 1) * cap, :], (((1,), (1,)), ((), ())),
+            precision=lax.Precision.HIGHEST, preferred_element_type=F32)
+    t_copy = []
+    for r in range(1, tp):
+        t_copy.append(start(rdma(
+            dsend, drecv.at[r - 1], dts.at[r - 1], dtr.at[r - 1], me_e, lax.rem(me_t + r, tp))))
+
+    own = piece(me_t)
+    b_copy[3].wait_recv()
+    mine[...] = own + rsib[3].astype(F32)
+    dots = dsend[...]
+    for copy_index, copy in enumerate(t_copy):
+        copy.wait_recv()
+        dots = dots + drecv[copy_index]
+    dsum[...] = dots
+    dz_copy = []
+    for r in range(1, ep):
+        to = lax.rem(me_e + r, ep)
+        dz_copy.append(start(rdma(
+            dsum.at[to], dback.at[me_e], dzs.at[r - 1], dzr.at[r - 1], to, me_t)))
+    dback[me_e] = dsum[me_e]
+
+    zb_copy = []
+    for r in order:
+        to = lax.rem(me_e + r, ep)
+        at = rows_of(to)
+        total = mine[at, :]
+        for q in range(3):
+            r_copy[r, q].wait_recv()
+            total = total + rown[q, at, :].astype(F32)
+        tsum[at, :] = total.astype(BF16)
+        if r:
+            zb_copy.append(start(rdma(
+                tsum.at[at], back.at[rows_of(me_e)], zbs.at[r - 1], zbr.at[r - 1], to, me_t)))
+        else:
+            back[at, :] = tsum[at, :]
+
+    for copy in dz_copy:
+        copy.wait_recv()
+    share = tok_dev // tp
+    first = pl.ds(pl.multiple_of(me_t * share, share), share)
+    slot_lane = lax.broadcasted_iota(jnp.int32, (share, cap), 1).astype(F32)
+    grads = []
+    for k in range(2):
+        want = dest_ref[k, first, 0:1]
+        total = jnp.zeros((share, 1), F32)
+        for s in range(ep):
+            hit = want == slot_lane + float(s * cap)
+            total = total + jnp.sum(
+                jnp.where(hit, dback[s, 0:1, :].astype(BF16).astype(F32), 0.0), axis=1, keepdims=True)
+        grads.append(total)
+    gg_ref[...] = jnp.concatenate(grads, axis=1) / gates_ref[first, :]
+
+    for copy in zb_copy:
+        copy.wait_recv()
+    tg_ref[...] = dot_nn(comb_ref[...], back[...]).astype(BF16)
+    for copy in sends:
+        copy.wait_send()
+    for copy in outs:
+        copy.wait()
+
+
+def weight_kernel(x_ref, c_ref, hid_ref, gp_ref, up_ref, gg_ref, ug_ref, dg_ref):
+    x = x_ref[...]
+    gg_ref[...] = dot_tn(x, gp_ref[...]).astype(BF16)
+    ug_ref[...] = dot_tn(x, up_ref[...]).astype(BF16)
+    dg_ref[...] = dot_tn(hid_ref[...], c_ref[...]).astype(BF16)
+
+
+def fused(tokens, out_grad, routes, gates, gate_weight, up_weight, down_weight):
+    tok_dev, top_k = routes.shape
+    ep = lax.axis_size("ep")
+    tp = lax.axis_size("tp")
+    cap = (3 * tok_dev + ep - 1) // ep
+    slots = ep * cap
+    dw = tokens.shape[1]
+    model = gate_weight.shape[1]
+    fw = gate_weight.shape[2]
+    share = tok_dev // tp
+    vmem = pl.BlockSpec(memory_space=pltpu.VMEM)
+    any_ = pl.BlockSpec(memory_space=pl.ANY)
+    dma = lambda n: pltpu.SemaphoreType.DMA((n,))
+    wide = jax.ShapeDtypeStruct((tp, slots, dw), BF16)
+    part = jax.ShapeDtypeStruct((slots, fw), BF16)
+    flops = 10 * slots * model * fw
+    tokens_grad, gates_grad, xs, cs, hid, gp, up = pl.pallas_call(
+        functools.partial(exchange_kernel, ep, tp, cap),
+        out_shape=(
+            jax.ShapeDtypeStruct((tok_dev, dw), BF16),
+            jax.ShapeDtypeStruct((share, top_k), F32),
+            wide, wide, part, part, part,
+        ),
+        in_specs=[vmem] * 4 + [any_] * 3,
+        out_specs=[vmem, vmem] + [any_] * 5,
+        scratch_shapes=[
+            pltpu.VMEM((model, fw), BF16),
+            pltpu.VMEM((model, fw), BF16),
+            pltpu.VMEM((fw, model), BF16),
+            pltpu.VMEM((slots, dw), BF16),
+            pltpu.VMEM((slots, dw), BF16),
+            pltpu.VMEM((tp, slots, dw), BF16),
+            pltpu.VMEM((tp, slots, dw), BF16),
+            pltpu.VMEM((tok_dev, slots), BF16),
+            pltpu.VMEM((2, tok_dev, 128), F32),
+            pltpu.VMEM((slots, fw), F32),
+            pltpu.VMEM((slots, fw), F32),
+            pltpu.VMEM((slots, fw), F32),
+            pltpu.VMEM((slots, fw), BF16),
+            pltpu.VMEM((slots, fw), BF16),
+            pltpu.VMEM((slots, fw), BF16),
+            pltpu.VMEM((4, slots, dw), BF16),
+            pltpu.VMEM((4, slots, dw), BF16),
+            pltpu.VMEM((3, slots, dw), BF16),
+            pltpu.VMEM((3, slots, dw), BF16),
+            pltpu.VMEM((slots, dw), F32),
+            pltpu.VMEM((slots, dw), BF16),
+            pltpu.VMEM((slots, dw), BF16),
+            pltpu.VMEM((ep, 8, cap), F32),
+            pltpu.VMEM((tp - 1, ep, 8, cap), F32),
+            pltpu.VMEM((ep, 8, cap), F32),
+            pltpu.VMEM((ep, 8, cap), F32),
+            dma(3), dma(5),
+            dma(2 * ep), dma(2 * ep), dma(4 * ep), dma(4 * ep), dma(2 * ep), dma(2 * ep),
+            dma(8 * ep), dma(8 * ep),
+            dma(4), dma(4), dma(3 * ep), dma(3 * ep), dma(ep), dma(ep),
+            dma(tp), dma(tp), dma(ep), dma(ep),
+        ],
+        compiler_params=pltpu.CompilerParams(
+            collective_id=0, has_side_effects=True, vmem_limit_bytes=VMEM_BYTES),
+        cost_estimate=pl.CostEstimate(flops=flops, bytes_accessed=6 * model * fw, transcendentals=0),
+    )(tokens, out_grad, routes, gates, gate_weight, up_weight, down_weight)
+    whole = pl.BlockSpec((slots, fw), lambda j: (0, 0))
+    slab = pl.BlockSpec((None, slots, dw), lambda j: (j, 0, 0))
+    tall = pl.BlockSpec((None, dw, fw), lambda j: (0, j, 0))
+    gate_grad, up_grad, down_grad = pl.pallas_call(
+        weight_kernel,
+        grid=(tp,),
+        out_shape=(
+            jax.ShapeDtypeStruct((1, model, fw), BF16),
+            jax.ShapeDtypeStruct((1, model, fw), BF16),
+            jax.ShapeDtypeStruct((1, fw, model), BF16),
+        ),
+        in_specs=[slab, slab, whole, whole, whole],
+        out_specs=[tall, tall, pl.BlockSpec((None, fw, dw), lambda j: (0, 0, j))],
+        compiler_params=pltpu.CompilerParams(vmem_limit_bytes=VMEM_BYTES),
+        cost_estimate=pl.CostEstimate(
+            flops=6 * slots * model * fw, bytes_accessed=6 * model * fw, transcendentals=0),
+    )(xs, cs, hid, gp, up)
+    return (tokens_grad, gates_grad, gate_grad, up_grad, down_grad)
+
+
+def fits_fused(ep, tp, tokens, routes, gate_weight):
+    cap = (3 * routes.shape[0] + ep - 1) // ep
+    return (
+        tp == 8 and 2 <= ep <= 8 and tp % ep == 0 and cap % 16 == 0 and cap <= 128
+        and tokens.shape[1] % 128 == 0 and routes.shape[1] == 2
+        and routes.shape[0] % (8 * tp) == 0
+        and gate_weight.shape[2] % 16 == 0
+    )
 
 
 def expert_grads(rows, cotan, w_gate, w_up, w_down):
@@ -26,6 +420,8 @@
     tok_dev, top_k = routes.shape
     ep_size = lax.axis_size("ep")
     tp_size = lax.axis_size("tp")
+    if fits_fused(ep_size, tp_size, tokens, routes, gate_weight):
+        return fused(tokens, out_grad, routes, gates, gate_weight, up_weight, down_weight)
     capacity = (3 * tok_dev + ep_size - 1) // ep_size
     buffer_rows = ep_size * capacity
     slice_width = tokens.shape[1]

time: 149 us -> 94.2 us (0.63)
  Pallas kernels: 0 us -> 73.3 us
  waiting for transfers between devices: 45.9 us -> 0 us
  blocking collectives: 36.7 us -> 0 us
  matrix products: 31.3 us -> 0 us
  between operations: 13.9 us -> 0.65 us
  local copies, waits for them, and re-layouts: 8.1 us -> 19.8 us
  starting transfers between devices: 9.33 us -> 0 us
  other arithmetic: 3.1 us -> 0 us
    pallas_call x0 -> x2, Pallas kernels: none -> 73.3 us  [the longest x1 63.3 us: fused(): pl.pallas_call(functools.partial(exchange_kernel, ep, tp, cap), out_shape...]
    all_gather x2 -> x0, waiting for transfers between devices: 35.1 us -> none  [the longest x1 20.8 us: on_device(): lax.all_gather(recv_cotan, 'tp', axis=2, tiled=True)]
    dot_general x11 -> x0, matrix products: 31.3 us -> none  [the longest x1 5.73 us: expert_grads(): hid_grad = jnp.dot(cotan, w_down.T, preferred_element_type=jnp.float32)]
    all_to_all x2 -> x0, blocking collectives: 23.6 us -> none  [the longest x1 13.7 us: on_device(): lax.all_to_all(sent_rows.reshape(ep_size, capacity, slice_width), 'ep', s...]
    unnamed x21 -> x14, local copies, waits for them, and re-layouts: 2.29 us -> 19.8 us
    psum x1 -> x0, blocking collectives: 13.1 us -> none  [on_device(): summed = lax.psum(slot_dots, 'tp')]
    reduce_scatter x1 -> x0, waiting for transfers between devices: 10.8 us -> none  [on_device(): lax.psum_scatter(partial_value.reshape(ep_size, capacity, model_width), '...]
    all_to_all x2 -> x0, starting transfers between devices: 9.21 us -> none  [the longest x1 4.6 us: on_device(): lax.all_to_all(summed.reshape(ep_size, capacity).astype(jnp.bfloat16), 'e...]
  transfers between devices with their start and end apart: 5 -> 0, of which waited for: 3 -> 0; matrix products, arithmetic and copies ran while one was open for 17% -> 0% of each run, Pallas kernels for 0% -> 0%
where the time goes in v1:
time: 94.2 us; the launch traced here: 93.7 us
  Pallas kernels  73.3 us (78%)
  local copies, waits for them, and re-layouts  19.8 us (21%)
    pallas_call x1, Pallas kernels, fused(): pl.pallas_call(functools.partial(exchange_kernel, ep, tp, cap), out_shape...  63.3 us
    unnamed x14, local copies, waits for them, and re-layouts  19.8 us
    pallas_call x1, Pallas kernels, fused(): pl.pallas_call(weight_kernel, grid=(tp,), out_shape=(jax.ShapeDtypeStruct...  9.98 us

profile of v1, /device:TPU:0, one launch (start us, length us, event | category | flops | bytes accessed | tf_op | source)
XLA Modules:
  0.0 93.7 jit_solution(2270306263536575551)
XLA Ops:
  0.6 1.4 %copy.12.routes_ref = s32[128,2]{1,0:T(8,128)} copy(s32[128,2]{0,1:T(2,128)} %param.9) | data formatting | bytes 2048 | tf_op args[2]
  2.0 1.4 %copy.13.gates_ref = f32[128,2]{1,0:T(8,128)} copy(f32[128,2]{0,1:T(2,128)} %param.10) | data formatting | bytes 2048 | tf_op args[3]
  3.5 0.0 copy-start.1
  3.5 4.7 %copy.14.wg_hbm = bf16[1,2048,704]{2,1,0:T(8,128)(2,1)} copy(bf16[1,2048,704]{1,2,0:T(8,128)(2,1)} %param.11) | data formatting | bytes 5767168 | tf_op args[4]
  8.2 0.0 copy-done.1
  8.2 2.8 %copy.15.wu_hbm = bf16[1,2048,704]{2,1,0:T(8,128)(2,1)} copy(bf16[1,2048,704]{1,2,0:T(8,128)(2,1)S(1)} %copy-done.1) | data formatting | bytes 5767168 | tf_op args[5]
  11.0 63.3 %shard_map.110 = (bf16[128,256]{1,0:T(8,128)(2,1)}, f32[16,2]{1,0:T(8,128)}, bf16[8,384,256]{2,1,0:T(8,128)(2,1)}, bf16[8,384,256]{2,1,0:T(8,128)(2,1)}, bf16[38...) custom-call(bf16[128,256]{1,0:T(8,128)(2,1)} %tok_ref.1, bf16[128,256]{1,0:T(8,128)(2,1)} %og_ref.1, ...), custom_call_target="tpu_custom_call" | custom-call | flops 5536481280 | bytes 8650752 | tf_op jit(solution)/shard_map/pallas_call | solution.py:325
  74.3 1.3 %copy.16 = f32[16,2]{0,1:T(2,128)} copy(f32[16,2]{1,0:T(8,128)} %get-tuple-element.26) | data formatting | bytes 256
  75.6 10.0 %shard_map.111 = (bf16[1,2048,704]{2,1,0:T(8,128)(2,1)}, bf16[1,2048,704]{2,1,0:T(8,128)(2,1)}, bf16[1,704,2048]{2,1,0:T(8,128)(2,1)}) custom-call(bf16[8,384,256]{2,1,0:T(8,128)(2,1)} %get-tuple-element.17.x_ref, bf16[8,384,256]{2,1,0:T(8,128)(2,1)} %get-tuple-element.18.c_ref, bf16[384,704]{1,0:T(8,128)(2,1)} %get-tuple-element.19.hid_ref, ...), custom_call_target="tpu_custom_call" | custom-call | flops 3321888768 | bytes 8650752 | tf_op jit(solution)/shard_map/pallas_call | solution.py:374
  85.6 0.0 copy-start
  85.6 4.7 %copy.17 = bf16[1,2048,704]{1,2,0:T(8,128)(2,1)} copy(bf16[1,2048,704]{2,1,0:T(8,128)(2,1)} %get-tuple-element.27) | data formatting | bytes 5767168
  90.3 0.0 copy-done
  90.3 0.0 copy-start.2
  90.3 2.7 %copy.18 = bf16[1,2048,704]{1,2,0:T(8,128)(2,1)} copy(bf16[1,2048,704]{2,1,0:T(8,128)(2,1)S(1)} %copy-done) | data formatting | bytes 5767168
  93.0 0.0 copy-done.2
  93.0 0.6 copy.20
Async XLA Ops:
  3.5 4.7 %copy-start.1 = (bf16[1,2048,704]{1,2,0:T(8,128)(2,1)S(1)}, bf16[1,2048,704]{1,2,0:T(8,128)(2,1)}, u32[]{:S(2)}) copy-start(bf16[1,2048,704]{1,2,0:T(8,128)(2,1)} %param.12) | copy-start | bytes 8650756
  85.6 4.7 %copy-start = (bf16[1,2048,704]{2,1,0:T(8,128)(2,1)S(1)}, bf16[1,2048,704]{2,1,0:T(8,128)(2,1)}, u32[]{:S(2)}) copy-start(bf16[1,2048,704]{2,1,0:T(8,128)(2,1)} %get-tuple-element.28) | copy-start | bytes 8650756
  90.3 2.7 %copy-start.2 = (bf16[128,256]{1,0:T(8,128)(2,1)S(1)}, bf16[128,256]{1,0:T(8,128)(2,1)}, u32[]{:S(2)}) copy-start(bf16[128,256]{1,0:T(8,128)(2,1)} %get-tuple-element.35) | copy-start | bytes 196612

commit v2 on v1

--- a/solution.py
+++ b/solution.py
@@ -33,8 +33,8 @@
     ep, tp, cap,
     tok_ref, og_ref, routes_ref, gates_ref, wg_hbm, wu_hbm, wd_hbm,
     tg_ref, gg_ref, xo_hbm, co_hbm, ho_hbm, gpo_hbm, upo_hbm,
-    wg, wu, wd, sx, sc, xs, cs, comb_ref, dest_ref,
-    pg, pu, hg, hid, gp, up,
+    wg, wu, wd, sx, sc, xs, cs, comb_ref, pick_ref,
+    pg, pu, hg, hid, gp, up, hid_t, gp_t, up_t,
     psib, rsib, pown, rown, mine, tsum, back, dsend, drecv, dsum, dback,
     wsem, osem,
     zs, zr, ns, nr, ds_, dr, ss, sr,
@@ -47,7 +47,7 @@
     diag = flip(nbr[0], 4)
     slots = ep * cap
     tok_dev, dw = tok_ref.shape
-    fw = wg.shape[1]
+    fw = wg.shape[0]
 
     def rdma(src, dst, s_sem, r_sem, e, t):
         return pltpu.make_async_remote_copy(
@@ -70,29 +70,29 @@
         pl.semaphore_signal(
             barrier, inc=1, device_id={"ep": me_e, "tp": lax.rem(me_t + r, tp)}, device_id_type=MESH)
 
-    expert = [routes_ref[:, k : k + 1].astype(F32) for k in range(2)]
-    lane = lax.broadcasted_iota(jnp.int32, (tok_dev, 128), 1).astype(F32)
-    oh = [jnp.where(expert[k] == lane, 1.0, 0.0) for k in range(2)]
+    expert = [routes_ref[k : k + 1, :].astype(F32) for k in range(2)]
+    group = lax.broadcasted_iota(jnp.int32, (16, tok_dev), 0).astype(F32)
+    oh = [jnp.where(expert[k] == group, 1.0, 0.0) for k in range(2)]
     row_id = lax.broadcasted_iota(jnp.int32, (tok_dev, tok_dev), 0)
     col_id = lax.broadcasted_iota(jnp.int32, (tok_dev, tok_dev), 1)
-    below = jnp.where(col_id < row_id, 1.0, 0.0).astype(BF16)
-    before = dot_nn(below, (oh[0] + oh[1]).astype(BF16))
+    above = jnp.where(row_id < col_id, 1.0, 0.0).astype(BF16)
+    before = dot_nn((oh[0] + oh[1]).astype(BF16), above)
     rank = [
-        jnp.sum(before * oh[0], axis=1, keepdims=True),
-        jnp.sum((before + oh[0]) * oh[1], axis=1, keepdims=True),
+        jnp.sum(before * oh[0], axis=0, keepdims=True),
+        jnp.sum((before + oh[0]) * oh[1], axis=0, keepdims=True),
     ]
-    slot_id = lax.broadcasted_iota(jnp.int32, (tok_dev, slots), 1).astype(F32)
-    dest = [expert[k] * float(cap) + rank[k] for k in range(2)]
-    comb = [jnp.where(dest[k] == slot_id, 1.0, 0.0) for k in range(2)]
-    both = (comb[0] + comb[1]).astype(BF16)
-    comb_ref[...] = both
+    slot_id = lax.broadcasted_iota(jnp.int32, (slots, tok_dev), 0).astype(F32)
+    slot_gate = jnp.zeros((slots, 1), F32)
+    both = jnp.zeros((slots, tok_dev), F32)
     for k in range(2):
-        dest_ref[k] = jnp.broadcast_to(dest[k], (tok_dev, 128))
-    sx[...] = dot_tn(both, tok_ref[...]).astype(BF16)
-    og = og_ref[...].astype(F32)
-    scaled = jnp.concatenate([(gates_ref[:, k : k + 1] * og).astype(BF16) for k in range(2)], axis=0)
-    picks = jnp.concatenate([comb[0], comb[1]], axis=0).astype(BF16)
-    sc[...] = dot_tn(picks, scaled).astype(BF16)
+        pick = jnp.where(expert[k] * float(cap) + rank[k] == slot_id, 1.0, 0.0)
+        pick_ref[k] = pick
+        both = both + pick
+        slot_gate = slot_gate + jnp.sum(pick * gates_ref[k : k + 1, :], axis=1, keepdims=True)
+    select = both.astype(BF16)
+    comb_ref[...] = select
+    sx[...] = dot_nn(select, tok_ref[...]).astype(BF16)
+    sc[...] = (slot_gate * dot_nn(select, og_ref[...])).astype(BF16)
 
     pl.semaphore_wait(barrier, ep - 1 + tp - 1)
 
@@ -158,8 +158,8 @@
         def _(j):
             part = pl.ds(pl.multiple_of(j * dw, dw), dw)
             x = xs[j]
-            pg[...] += dot_nn(x, wg[part, :])
-            pu[...] += dot_nn(x, wu[part, :])
+            pg[...] += dot_nt(x, wg[:, part])
+            pu[...] += dot_nt(x, wu[:, part])
 
     outs = []
 
@@ -209,13 +209,9 @@
         up[at, :] = (h * act).astype(BF16)
         pg[at, :] = hidden.astype(F32) * h
 
-    put(hid, ho_hbm, 2)
-    put(gp, gpo_hbm, 3)
-    put(up, upo_hbm, 4)
-
     def piece(t):
         part = pl.ds(pl.multiple_of(t * dw, dw), dw)
-        return dot_nt(gp[...], wg[part, :]) + dot_nt(up[...], wu[part, :])
+        return dot_nn(gp[...], wg[:, part]) + dot_nn(up[...], wu[:, part])
 
     chips = (diag, nbr[0], nbr[1], me_t)
     b_copy = []
@@ -244,6 +240,10 @@
         t_copy.append(start(rdma(
             dsend, drecv.at[r - 1], dts.at[r - 1], dtr.at[r - 1], me_e, lax.rem(me_t + r, tp))))
 
+    for k, (rows, flat, out) in enumerate(((hid, hid_t, ho_hbm), (gp, gp_t, gpo_hbm), (up, up_t, upo_hbm))):
+        flat[...] = rows[...].T
+        put(flat, out, 2 + k)
+
     own = piece(me_t)
     b_copy[3].wait_recv()
     mine[...] = own + rsib[3].astype(F32)
@@ -277,22 +277,22 @@
     for copy in dz_copy:
         copy.wait_recv()
     share = tok_dev // tp
-    first = pl.ds(pl.multiple_of(me_t * share, share), share)
-    slot_lane = lax.broadcasted_iota(jnp.int32, (share, cap), 1).astype(F32)
+    own_row = lax.broadcasted_iota(jnp.int32, (tok_dev, share), 0)
+    own_col = lax.broadcasted_iota(jnp.int32, (tok_dev, share), 1) + me_t * share
+    own_pick = jnp.where(own_row == own_col, 1.0, 0.0)
+    exact = dict(precision=lax.Precision.HIGHEST, preferred_element_type=F32)
     grads = []
     for k in range(2):
-        want = dest_ref[k, first, 0:1]
-        total = jnp.zeros((share, 1), F32)
+        total = jnp.zeros((8, tok_dev), F32)
         for s in range(ep):
-            hit = want == slot_lane + float(s * cap)
-            total = total + jnp.sum(
-                jnp.where(hit, dback[s, 0:1, :].astype(BF16).astype(F32), 0.0), axis=1, keepdims=True)
-        grads.append(total)
-    gg_ref[...] = jnp.concatenate(grads, axis=1) / gates_ref[first, :]
+            total = total + jnp.dot(dback[s], pick_ref[k, s * cap : (s + 1) * cap, :], **exact)
+        grads.append(total[0:1, :] / gates_ref[k : k + 1, :])
+    shares = jnp.concatenate([*grads, jnp.zeros((6, tok_dev), F32)], axis=0)
+    gg_ref[...] = jnp.dot(shares, own_pick, **exact)[0:2, :]
 
     for copy in zb_copy:
         copy.wait_recv()
-    tg_ref[...] = dot_nn(comb_ref[...], back[...]).astype(BF16)
+    tg_ref[...] = dot_tn(comb_ref[...], back[...]).astype(BF16)
     for copy in sends:
         copy.wait_send()
     for copy in outs:
@@ -301,9 +301,9 @@
 
 def weight_kernel(x_ref, c_ref, hid_ref, gp_ref, up_ref, gg_ref, ug_ref, dg_ref):
     x = x_ref[...]
-    gg_ref[...] = dot_tn(x, gp_ref[...]).astype(BF16)
-    ug_ref[...] = dot_tn(x, up_ref[...]).astype(BF16)
-    dg_ref[...] = dot_tn(hid_ref[...], c_ref[...]).astype(BF16)
+    gg_ref[...] = dot_nn(gp_ref[...], x).astype(BF16)
+    ug_ref[...] = dot_nn(up_ref[...], x).astype(BF16)
+    dg_ref[...] = dot_nn(hid_ref[...], c_ref[...]).astype(BF16)
 
 
 def fused(tokens, out_grad, routes, gates, gate_weight, up_weight, down_weight):
@@ -320,33 +320,36 @@
     any_ = pl.BlockSpec(memory_space=pl.ANY)
     dma = lambda n: pltpu.SemaphoreType.DMA((n,))
     wide = jax.ShapeDtypeStruct((tp, slots, dw), BF16)
-    part = jax.ShapeDtypeStruct((slots, fw), BF16)
+    part = jax.ShapeDtypeStruct((fw, slots), BF16)
     flops = 10 * slots * model * fw
     tokens_grad, gates_grad, xs, cs, hid, gp, up = pl.pallas_call(
         functools.partial(exchange_kernel, ep, tp, cap),
         out_shape=(
             jax.ShapeDtypeStruct((tok_dev, dw), BF16),
-            jax.ShapeDtypeStruct((share, top_k), F32),
+            jax.ShapeDtypeStruct((top_k, share), F32),
             wide, wide, part, part, part,
         ),
         in_specs=[vmem] * 4 + [any_] * 3,
         out_specs=[vmem, vmem] + [any_] * 5,
         scratch_shapes=[
-            pltpu.VMEM((model, fw), BF16),
-            pltpu.VMEM((model, fw), BF16),
+            pltpu.VMEM((fw, model), BF16),
+            pltpu.VMEM((fw, model), BF16),
             pltpu.VMEM((fw, model), BF16),
             pltpu.VMEM((slots, dw), BF16),
             pltpu.VMEM((slots, dw), BF16),
             pltpu.VMEM((tp, slots, dw), BF16),
             pltpu.VMEM((tp, slots, dw), BF16),
-            pltpu.VMEM((tok_dev, slots), BF16),
-            pltpu.VMEM((2, tok_dev, 128), F32),
+            pltpu.VMEM((slots, tok_dev), BF16),
+            pltpu.VMEM((2, slots, tok_dev), F32),
             pltpu.VMEM((slots, fw), F32),
             pltpu.VMEM((slots, fw), F32),
             pltpu.VMEM((slots, fw), F32),
             pltpu.VMEM((slots, fw), BF16),
             pltpu.VMEM((slots, fw), BF16),
             pltpu.VMEM((slots, fw), BF16),
+            pltpu.VMEM((fw, slots), BF16),
+            pltpu.VMEM((fw, slots), BF16),
+            pltpu.VMEM((fw, slots), BF16),
             pltpu.VMEM((4, slots, dw), BF16),
             pltpu.VMEM((4, slots, dw), BF16),
             pltpu.VMEM((3, slots, dw), BF16),
@@ -367,25 +370,26 @@
         compiler_params=pltpu.CompilerParams(
             collective_id=0, has_side_effects=True, vmem_limit_bytes=VMEM_BYTES),
         cost_estimate=pl.CostEstimate(flops=flops, bytes_accessed=6 * model * fw, transcendentals=0),
-    )(tokens, out_grad, routes, gates, gate_weight, up_weight, down_weight)
-    whole = pl.BlockSpec((slots, fw), lambda j: (0, 0))
+    )(tokens, out_grad, routes.T, gates.T, jnp.swapaxes(gate_weight, 1, 2),
+      jnp.swapaxes(up_weight, 1, 2), down_weight)
+    whole = pl.BlockSpec((fw, slots), lambda j: (0, 0))
     slab = pl.BlockSpec((None, slots, dw), lambda j: (j, 0, 0))
-    tall = pl.BlockSpec((None, dw, fw), lambda j: (0, j, 0))
+    tall = pl.BlockSpec((None, fw, dw), lambda j: (0, 0, j))
     gate_grad, up_grad, down_grad = pl.pallas_call(
         weight_kernel,
         grid=(tp,),
         out_shape=(
-            jax.ShapeDtypeStruct((1, model, fw), BF16),
-            jax.ShapeDtypeStruct((1, model, fw), BF16),
+            jax.ShapeDtypeStruct((1, fw, model), BF16),
+            jax.ShapeDtypeStruct((1, fw, model), BF16),
             jax.ShapeDtypeStruct((1, fw, model), BF16),
         ),
         in_specs=[slab, slab, whole, whole, whole],
-        out_specs=[tall, tall, pl.BlockSpec((None, fw, dw), lambda j: (0, 0, j))],
+        out_specs=[tall, tall, tall],
         compiler_params=pltpu.CompilerParams(vmem_limit_bytes=VMEM_BYTES),
         cost_estimate=pl.CostEstimate(
             flops=6 * slots * model * fw, bytes_accessed=6 * model * fw, transcendentals=0),
     )(xs, cs, hid, gp, up)
-    return (tokens_grad, gates_grad, gate_grad, up_grad, down_grad)
+    return (tokens_grad, gates_grad.T, jnp.swapaxes(gate_grad, 1, 2), jnp.swapaxes(up_grad, 1, 2), down_grad)
 
 
 def fits_fused(ep, tp, tokens, routes, gate_weight):

time: 94.2 us -> 75.8 us (0.80)
  local copies, waits for them, and re-layouts: 19.8 us -> 1.2 us
    unnamed x14 -> x6, local copies, waits for them, and re-layouts: 19.8 us -> 1.2 us
where the time goes in v2:
time: 75.8 us; the launch traced here: 75.5 us
  Pallas kernels  73.7 us (97%)
  local copies, waits for them, and re-layouts  1.2 us (2%)
    pallas_call x1, Pallas kernels, fused(): pl.pallas_call(functools.partial(exchange_kernel, ep, tp, cap), out_shape...  63.3 us
    pallas_call x1, Pallas kernels, fused(): pl.pallas_call(weight_kernel, grid=(tp,), out_shape=(jax.ShapeDtypeStruct...  10.4 us

profile of v2, /device:TPU:0, one launch (start us, length us, event | category | flops | bytes accessed | tf_op | source)
XLA Modules:
  0.0 75.5 jit_solution(15143689148370965325)
XLA Ops:
  0.6 63.3 %shard_map.110 = (bf16[128,256]{1,0:T(8,128)(2,1)}, f32[2,16]{1,0:T(2,128)}, bf16[8,384,256]{2,1,0:T(8,128)(2,1)}, bf16[8,384,256]{2,1,0:T(8,128)(2,1)}, bf16[70...) custom-call(bf16[128,256]{1,0:T(8,128)(2,1)} %tok_ref.1, bf16[128,256]{1,0:T(8,128)(2,1)} %og_ref.1, ...), custom_call_target="tpu_custom_call" | custom-call | flops 5536481280 | bytes 8650752 | tf_op jit(solution)/shard_map/pallas_call | solution.py:325
  63.9 0.0 copy-start
  63.9 0.0 copy-start.1
  63.9 10.4 %shard_map.111 = (bf16[1,704,2048]{2,1,0:T(8,128)(2,1)}, bf16[1,704,2048]{2,1,0:T(8,128)(2,1)}, bf16[1,704,2048]{2,1,0:T(8,128)(2,1)}) custom-call(bf16[8,384,256]{2,1,0:T(8,128)(2,1)} %get-tuple-element.17.x_ref, bf16[8,384,256]{2,1,0:T(8,128)(2,1)} %get-tuple-element.18.c_ref, bf16[704,384]{1,0:T(8,128)(2,1)} %get-tuple-element.19.hid_ref, ...), custom_call_target="tpu_custom_call" | custom-call | flops 3321888768 | bytes 8650752 | tf_op jit(solution)/shard_map/pallas_call | solution.py:378
  74.3 0.0 copy-done
  74.3 0.6 copy.14
  74.9 0.0 copy-done.1
  75.0 0.6 copy.15
Async XLA Ops:
  63.9 10.4 %copy-start = (bf16[128,256]{1,0:T(8,128)(2,1)S(1)}, bf16[128,256]{1,0:T(8,128)(2,1)}, u32[]{:S(2)}) copy-start(bf16[128,256]{1,0:T(8,128)(2,1)} %get-tuple-element.30) | copy-start | bytes 196612
  63.9 11.0 %copy-start.1 = (f32[2,16]{1,0:T(2,128)S(1)}, f32[2,16]{1,0:T(2,128)}, u32[]{:S(2)}) copy-start(f32[2,16]{1,0:T(2,128)} %get-tuple-element.16) | copy-start | bytes 388

commit v3 on v2

--- a/solution.py
+++ b/solution.py
@@ -213,6 +213,22 @@
         part = pl.ds(pl.multiple_of(t * dw, dw), dw)
         return dot_nn(gp[...], wg[:, part]) + dot_nn(up[...], wu[:, part])
 
+    ones = jnp.ones((8, fw), F32)
+    tile_row = lax.broadcasted_iota(jnp.int32, (8, 128), 0)
+    tile = jnp.zeros((8, 128), F32)
+    for s in range(ep):
+        sums = lax.dot_general(
+            ones, pg[s * cap : (s + 1) * cap, :], (((1,), (1,)), ((), ())),
+            precision=lax.Precision.HIGHEST, preferred_element_type=F32)
+        if cap < 128:
+            sums = jnp.concatenate([sums, jnp.zeros((8, 128 - cap), F32)], axis=1)
+        tile = jnp.where(tile_row == s, sums, tile)
+    dsend[...] = tile
+    t_copy = []
+    for r in range(1, tp):
+        t_copy.append(start(rdma(
+            dsend, drecv.at[r - 1], dts.at[r - 1], dtr.at[r - 1], me_e, lax.rem(me_t + r, tp))))
+
     chips = (diag, nbr[0], nbr[1], me_t)
     b_copy = []
     for q in range(4):
@@ -230,23 +246,6 @@
             r_copy[r, q] = start(rdma(
                 pown.at[q, at], rown.at[q, at], rs.at[r * 3 + q], rr.at[r * 3 + q], me_e, chips[q]))
 
-    ones = jnp.ones((8, fw), F32)
-    for s in range(ep):
-        dsend[s] = lax.dot_general(
-            ones, pg[s * cap : (s + 1) * cap, :], (((1,), (1,)), ((), ())),
-            precision=lax.Precision.HIGHEST, preferred_element_type=F32)
-    t_copy = []
-    for r in range(1, tp):
-        t_copy.append(start(rdma(
-            dsend, drecv.at[r - 1], dts.at[r - 1], dtr.at[r - 1], me_e, lax.rem(me_t + r, tp))))
-
-    for k, (rows, flat, out) in enumerate(((hid, hid_t, ho_hbm), (gp, gp_t, gpo_hbm), (up, up_t, upo_hbm))):
-        flat[...] = rows[...].T
-        put(flat, out, 2 + k)
-
-    own = piece(me_t)
-    b_copy[3].wait_recv()
-    mine[...] = own + rsib[3].astype(F32)
     dots = dsend[...]
     for copy_index, copy in enumerate(t_copy):
         copy.wait_recv()
@@ -255,10 +254,16 @@
     dz_copy = []
     for r in range(1, ep):
         to = lax.rem(me_e + r, ep)
-        dz_copy.append(start(rdma(
-            dsum.at[to], dback.at[me_e], dzs.at[r - 1], dzr.at[r - 1], to, me_t)))
-    dback[me_e] = dsum[me_e]
-
+        dz_copy.append(start(rdma(dsum, dback.at[me_e], dzs.at[r - 1], dzr.at[r - 1], to, me_t)))
+    dback[me_e] = dots
+
+    for k, (rows, flat, out) in enumerate(((hid, hid_t, ho_hbm), (gp, gp_t, gpo_hbm), (up, up_t, upo_hbm))):
+        flat[...] = rows[...].T
+        put(flat, out, 2 + k)
+
+    own = piece(me_t)
+    b_copy[3].wait_recv()
+    mine[...] = own + rsib[3].astype(F32)
     zb_copy = []
     for r in order:
         to = lax.rem(me_e + r, ep)
@@ -281,12 +286,14 @@
     own_col = lax.broadcasted_iota(jnp.int32, (tok_dev, share), 1) + me_t * share
     own_pick = jnp.where(own_row == own_col, 1.0, 0.0)
     exact = dict(precision=lax.Precision.HIGHEST, preferred_element_type=F32)
+    mine_row = lax.broadcasted_iota(jnp.int32, (8, 128), 0) == me_e
     grads = []
     for k in range(2):
         total = jnp.zeros((8, tok_dev), F32)
         for s in range(ep):
-            total = total + jnp.dot(dback[s], pick_ref[k, s * cap : (s + 1) * cap, :], **exact)
-        grads.append(total[0:1, :] / gates_ref[k : k + 1, :])
+            held = jnp.where(mine_row, dback[s], 0.0)[:, 0:cap]
+            total = total + jnp.dot(held, pick_ref[k, s * cap : (s + 1) * cap, :], **exact)
+        grads.append(jnp.sum(total, axis=0, keepdims=True) / gates_ref[k : k + 1, :])
     shares = jnp.concatenate([*grads, jnp.zeros((6, tok_dev), F32)], axis=0)
     gg_ref[...] = jnp.dot(shares, own_pick, **exact)[0:2, :]
 
@@ -357,10 +364,10 @@
             pltpu.VMEM((slots, dw), F32),
             pltpu.VMEM((slots, dw), BF16),
             pltpu.VMEM((slots, dw), BF16),
-            pltpu.VMEM((ep, 8, cap), F32),
-            pltpu.VMEM((tp - 1, ep, 8, cap), F32),
-            pltpu.VMEM((ep, 8, cap), F32),
-            pltpu.VMEM((ep, 8, cap), F32),
+            pltpu.VMEM((8, 128), F32),
+            pltpu.VMEM((tp - 1, 8, 128), F32),
+            pltpu.VMEM((8, 128), F32),
+            pltpu.VMEM((ep, 8, 128), F32),
             dma(3), dma(5),
             dma(2 * ep), dma(2 * ep), dma(4 * ep), dma(4 * ep), dma(2 * ep), dma(2 * ep),
             dma(8 * ep), dma(8 * ep),

time: 75.8 us -> 70.5 us (0.930)
  Pallas kernels: 73.7 us -> 68.3 us
    pallas_call x1, Pallas kernels: 63.3 us -> 57.9 us  [fused(): pl.pallas_call(functools.partial(exchange_kernel, ep, tp, cap), out_shape...]
where the time goes in v3:
time: 70.5 us; the launch traced here: 70.2 us
  Pallas kernels  68.3 us (97%)
  local copies, waits for them, and re-layouts  1.2 us (2%)
    pallas_call x1, Pallas kernels, fused(): pl.pallas_call(functools.partial(exchange_kernel, ep, tp, cap), out_shape...  57.9 us
    pallas_call x1, Pallas kernels, fused(): pl.pallas_call(weight_kernel, grid=(tp,), out_shape=(jax.ShapeDtypeStruct...  10.4 us

profile of v3, /device:TPU:0, one launch (start us, length us, event | category | flops | bytes accessed | tf_op | source)
XLA Modules:
  0.0 70.2 jit_solution(14166418024181531467)
XLA Ops:
  0.6 57.9 %shard_map.110 = (bf16[128,256]{1,0:T(8,128)(2,1)}, f32[2,16]{1,0:T(2,128)}, bf16[8,384,256]{2,1,0:T(8,128)(2,1)}, bf16[8,384,256]{2,1,0:T(8,128)(2,1)}, bf16[70...) custom-call(bf16[128,256]{1,0:T(8,128)(2,1)} %tok_ref.1, bf16[128,256]{1,0:T(8,128)(2,1)} %og_ref.1, ...), custom_call_target="tpu_custom_call" | custom-call | flops 5536481280 | bytes 8650752 | tf_op jit(solution)/shard_map/pallas_call | solution.py:332
  58.6 0.0 copy-start
  58.6 0.0 copy-start.1
  58.6 10.4 %shard_map.111 = (bf16[1,704,2048]{2,1,0:T(8,128)(2,1)}, bf16[1,704,2048]{2,1,0:T(8,128)(2,1)}, bf16[1,704,2048]{2,1,0:T(8,128)(2,1)}) custom-call(bf16[8,384,256]{2,1,0:T(8,128)(2,1)} %get-tuple-element.17.x_ref, bf16[8,384,256]{2,1,0:T(8,128)(2,1)} %get-tuple-element.18.c_ref, bf16[704,384]{1,0:T(8,128)(2,1)} %get-tuple-element.19.hid_ref, ...), custom_call_target="tpu_custom_call" | custom-call | flops 3321888768 | bytes 8650752 | tf_op jit(solution)/shard_map/pallas_call | solution.py:385
  69.0 0.0 copy-done
  69.0 0.6 copy.14
  69.6 0.0 copy-done.1
  69.6 0.6 copy.15
Async XLA Ops:
  58.6 10.4 %copy-start = (bf16[128,256]{1,0:T(8,128)(2,1)S(1)}, bf16[128,256]{1,0:T(8,128)(2,1)}, u32[]{:S(2)}) copy-start(bf16[128,256]{1,0:T(8,128)(2,1)} %get-tuple-element.30) | copy-start | bytes 196612
  58.6 11.0 %copy-start.1 = (f32[2,16]{1,0:T(2,128)S(1)}, f32[2,16]{1,0:T(2,128)}, u32[]{:S(2)}) copy-start(f32[2,16]{1,0:T(2,128)} %get-tuple-element.16) | copy-start | bytes 388
